TPU v7x, 32 devices: a whole 2x2x4 slice. The times are simulated.
32 devices in a mesh: ep: 32 (over z, y, x, core).
Axes of the slice: x: 2, y: 2, z: 4, core: 2. Of those that a mesh axis runs over, the one named last changes fastest.
Arguments:
- tokens: bfloat16 [512, 2048], P('ep'), may hold values from -6 to 6
- state: float32 [2, 512, 2048], P(None, 'ep'), may hold values from -4 to 4
- norm_mix: float32 [2048], replicated, may hold values from 0.1 to 1.9
- w_drive: bfloat16 [2048, 512], replicated, may hold values from -0.125 to 0.125
- lam_real: float32 [32, 64], replicated, may hold values from -1 to -0.05
- lam_imag: float32 [32, 64], replicated, may hold values from -3 to 3
- log_step: float32 [32], replicated, may hold values from -2.5 to 0.5
- b_real: float32 [32, 64, 16], replicated, may hold values from -1 to 1
- b_imag: float32 [32, 64, 16], replicated, may hold values from -1 to 1
- readout_real: float32 [32, 16, 64], replicated, may hold values from -0.5 to 0.5
- readout_imaginary: float32 [32, 16, 64], replicated, may hold values from -0.5 to 0.5
- d_skip: float32 [512], replicated, may hold values from -4 to 4
- w_value: bfloat16 [512, 512], replicated, may hold values from -0.25 to 0.25
- w_glugate: bfloat16 [512, 512], replicated, may hold values from -0.25 to 0.25
- w_output: bfloat16 [512, 2048], replicated, may hold values from -0.25 to 0.25
- norm_ffn: float32 [2048], replicated, may hold values from 0.1 to 1.9
- w_group: bfloat16 [2048, 4], replicated, may hold values from -0.125 to 0.125
- w_expert: bfloat16 [2048, 32], replicated, may hold values from -0.125 to 0.125
- route_ids: int32 [512, 6], P('ep'), may hold values from 0 to 31, all different within a row; in each aligned block of 16 rows (0 to 15, 16 to 31, ...) at most 7 rows name the same one
- expert_gate: bfloat16 [32, 2048, 512], P('ep'), may hold values from -0.125 to 0.125
- expert_up: bfloat16 [32, 2048, 512], P('ep'), may hold values from -0.125 to 0.125
- expert_down: bfloat16 [32, 512, 2048], P('ep'), may hold values from -1 to 1
- dense_vector: float32 [2048], replicated, may hold values from -0.125 to 0.125
- dense_gate: bfloat16 [2048, 8192], P(None, 'ep'), may hold values from -0.125 to 0.125
- dense_up: bfloat16 [2048, 8192], P(None, 'ep'), may hold values from -0.125 to 0.125
- dense_down: bfloat16 [8192, 2048], P('ep'), may hold values from -0.25 to 0.25
Outputs:
- layer_out: bfloat16 [512, 2048], P('ep')
- new_state: float32 [2, 512, 2048], P(None, 'ep')
Inputs may be any that keep to these rules, and one draw needn't show every extreme that they name: `route_ids`: each row names 6 different experts. Among the rows of one device no expert is named more than 7 times, a bound that some block reaches.
All inputs are finite; a program needn't handle non-finite values.
Results may differ from a plain program's by a relative error of at most 0.018.
Values may be sent and summed in bfloat16 or wider, within the bound.
A program may use at most 128 MiB of HBM per device.

v0:
```python
import jax
import jax.numpy as jnp
from jax import lax
from jax.sharding import PartitionSpec as P

EPS = 1e-05
HIGH_PRECISION = lax.Precision.HIGHEST


def rms_scale(values, gain):
    widened = values.astype(jnp.float32)
    scaled = widened * lax.rsqrt(jnp.mean(widened * widened, axis=-1, keepdims=True) + EPS)
    return (scaled * gain).astype(jnp.bfloat16)


def state_mixer(
    tokens,
    state,
    norm_mix,
    w_drive,
    lam_real,
    lam_imag,
    log_step,
    b_real,
    b_imag,
    readout_real,
    readout_imaginary,
    d_skip,
    w_value,
    w_glugate,
    w_output,
):
    row_count = tokens.shape[0]
    group_count, state_dimension = lam_real.shape
    channels = b_real.shape[2]
    normed_in = rms_scale(tokens, norm_mix)
    drive = jnp.dot(normed_in, w_drive, preferred_element_type=jnp.float32).astype(jnp.bfloat16)
    time_step = jnp.exp(log_step)[:, None]
    magnitude = jnp.exp(lam_real * time_step)
    decay_re = magnitude * jnp.cos(lam_imag * time_step)
    decay_im = magnitude * jnp.sin(lam_imag * time_step)
    modulus = lam_real * lam_real + lam_imag * lam_imag
    factor_re = ((decay_re - 1.0) * lam_real + decay_im * lam_imag) / modulus
    factor_im = (decay_im * lam_real - (decay_re - 1.0) * lam_imag) / modulus
    map_re = factor_re[:, :, None] * b_real - factor_im[:, :, None] * b_imag
    map_im = factor_re[:, :, None] * b_imag + factor_im[:, :, None] * b_real
    drive_wide = drive.astype(jnp.float32)
    grouped = drive_wide.reshape(row_count, group_count, channels)
    input_re = jnp.einsum("gpc,sgc->sgp", map_re, grouped, precision=HIGH_PRECISION)
    input_im = jnp.einsum("gpc,sgc->sgp", map_im, grouped, precision=HIGH_PRECISION)
    old_re = state[0].reshape(row_count, group_count, state_dimension)
    old_im = state[1].reshape(row_count, group_count, state_dimension)
    incoming_real = decay_re * old_re - decay_im * old_im + input_re
    incoming_imaginary = decay_re * old_im + decay_im * old_re + input_im
    projected_output = jnp.einsum(
        "xej,fxj->fxe", readout_real, incoming_real, precision=HIGH_PRECISION
    ) - jnp.einsum("xej,fxj->fxe", readout_imaginary, incoming_imaginary, precision=HIGH_PRECISION)
    readout = jax.nn.gelu(
        projected_output.reshape(row_count, group_count * channels) + d_skip * drive_wide
    ).astype(jnp.bfloat16)
    value_part = jnp.dot(readout, w_value, preferred_element_type=jnp.float32)
    gate_part = jnp.dot(readout, w_glugate, preferred_element_type=jnp.float32)
    mixed = (value_part * jax.nn.sigmoid(gate_part)).astype(jnp.bfloat16)
    resid = (
        tokens.astype(jnp.float32) + jnp.dot(mixed, w_output, preferred_element_type=jnp.float32)
    ).astype(jnp.bfloat16)
    new_state = jnp.stack(
        [incoming_real.reshape(row_count, -1), incoming_imaginary.reshape(row_count, -1)]
    )
    return (resid, new_state)


def route_gates(normed, w_group, w_expert, route_ids):
    row_count = normed.shape[0]
    group_count = w_group.shape[1]
    expert_count = w_expert.shape[1]
    per_group = expert_count // group_count
    group_exp = jnp.exp(jnp.dot(normed, w_group, preferred_element_type=jnp.float32))
    group_prob = group_exp / jnp.sum(group_exp, axis=1, keepdims=True)
    inner_exp = jnp.exp(jnp.dot(normed, w_expert, preferred_element_type=jnp.float32)).reshape(
        row_count, group_count, per_group
    )
    inner_prob = inner_exp / jnp.sum(inner_exp, axis=2, keepdims=True)
    joint = (group_prob[:, :, None] * inner_prob).reshape(row_count, expert_count)
    inner_flat = inner_prob.reshape(row_count, expert_count)
    matched = route_ids[:, :, None] == jnp.arange(expert_count, dtype=jnp.int32)[None, None, :]
    picked_joint = jnp.sum(jnp.where(matched, joint[:, None, :], 0.0), axis=2)
    picked_inner = jnp.sum(jnp.where(matched, inner_flat[:, None, :], 0.0), axis=2)
    return picked_joint / jnp.sum(picked_inner, axis=1, keepdims=True)


def expert_rows(rows_in, w_gate, w_up, w_down):
    gate_part = jnp.dot(rows_in, w_gate, preferred_element_type=jnp.float32)
    up_part = jnp.dot(rows_in, w_up, preferred_element_type=jnp.float32)
    hidden = (jax.nn.silu(gate_part) * up_part).astype(jnp.bfloat16)
    return jnp.dot(hidden, w_down, preferred_element_type=jnp.float32).astype(jnp.bfloat16)


def on_device(
    tokens,
    state,
    norm_mix,
    w_drive,
    lam_real,
    lam_imag,
    log_step,
    b_real,
    b_imag,
    readout_real,
    readout_imaginary,
    d_skip,
    w_value,
    w_glugate,
    w_output,
    norm_ffn,
    w_group,
    w_expert,
    route_ids,
    expert_gate,
    expert_up,
    expert_down,
    dense_vector,
    dense_gate,
    dense_up,
    dense_down,
):
    resid, new_state = state_mixer(
        tokens,
        state,
        norm_mix,
        w_drive,
        lam_real,
        lam_imag,
        log_step,
        b_real,
        b_imag,
        readout_real,
        readout_imaginary,
        d_skip,
        w_value,
        w_glugate,
        w_output,
    )
    normed = rms_scale(resid, norm_ffn)
    seq_count, width = normed.shape
    topk = route_ids.shape[1]
    expert_count = w_expert.shape[1]
    capacity = max(2, 5 * seq_count * topk // (2 * expert_count))
    own_gate = expert_gate[0]
    own_up = expert_up[0]
    own_down = expert_down[0]
    piece = lax.all_gather(normed, "ep", axis=0, tiled=True)
    branch_gate = jax.nn.sigmoid(
        jnp.dot(piece.astype(jnp.float32), dense_vector, precision=HIGH_PRECISION)
    )
    dense_g = jnp.dot(piece, dense_gate, preferred_element_type=jnp.float32)
    dense_u = jnp.dot(piece, dense_up, preferred_element_type=jnp.float32)
    hidden_all = (branch_gate[:, None] * jax.nn.silu(dense_g) * dense_u).astype(jnp.bfloat16)
    gates = route_gates(normed, w_group, w_expert, route_ids)
    flat_ids = route_ids.reshape(-1)
    onehot = (flat_ids[:, None] == jnp.arange(expert_count, dtype=jnp.int32)[None, :]).astype(
        jnp.int32
    )
    ordinal = jnp.sum((jnp.cumsum(onehot, axis=0) - 1) * onehot, axis=1)
    target = flat_ids * capacity + ordinal
    source_rows = jnp.repeat(normed, topk, axis=0)
    outgoing = jnp.zeros((expert_count * capacity, width), jnp.bfloat16).at[target].set(source_rows)
    outgoing = outgoing.reshape(expert_count, capacity, width)
    received = lax.all_to_all(outgoing, "ep", split_axis=0, concat_axis=0, tiled=True)
    senders, items, inner_width = received.shape
    result = expert_rows(received.reshape(senders * items, inner_width), own_gate, own_up, own_down)
    returned = lax.all_to_all(
        result.reshape(senders, items, inner_width), "ep", split_axis=0, concat_axis=0, tiled=True
    )
    picked = returned.reshape(expert_count * capacity, width)[target]
    weighted = picked.astype(jnp.float32).reshape(seq_count, topk, width) * gates[:, :, None]
    local_moe = jnp.sum(weighted, axis=1)
    summed = lax.psum_scatter(
        jnp.dot(hidden_all, dense_down, preferred_element_type=jnp.float32),
        "ep",
        scatter_dimension=0,
        tiled=True,
    )
    layer_out = (resid.astype(jnp.float32) + summed + local_moe).astype(jnp.bfloat16)
    return (layer_out, new_state)


def solution(mesh):
    placed = (
        P("ep", None),
        P(None, "ep", None),
        P(),
        P(),
        P(),
        P(),
        P(),
        P(),
        P(),
        P(),
        P(),
        P(),
        P(),
        P(),
        P(),
        P(),
        P(),
        P(),
        P("ep", None),
        P("ep", None, None),
        P("ep", None, None),
        P("ep", None, None),
        P(),
        P(None, "ep"),
        P(None, "ep"),
        P("ep", None),
    )
    return jax.shard_map(
        on_device,
        mesh=mesh,
        in_specs=placed,
        out_specs=(P("ep", None), P(None, "ep", None)),
        check_vma=False,
    )
```

profile of v0, /device:TPU:0, one launch (start us, length us, event | category | flops | bytes accessed | tf_op | source)
XLA Modules:
  0.0 244.7 jit_solution(4250216311229460943)
XLA Ops:
  7.3 1.3 exp.26
  8.6 1.0 fusion.49
  9.6 2.1 convolution_convert_fusion.1
  11.6 0.2 reshape.126
  11.8 0.1 reshape_squeeze.6
  11.9 0.1 reshape_squeeze.7
  12.1 0.9 cosine_multiply_fusion
  13.0 0.5 fusion.16
  13.6 0.5 fusion.17
  14.2 0.5 fusion.80
  14.7 0.5 fusion.15
  15.3 0.1 copy.56
  15.4 0.2 reshape.127
  15.6 0.2 fusion.81
  15.8 2.4 multiply_reduce_fusion.1
  18.3 0.7 multiply_convert_fusion
  19.1 59.0 %all-gather.2.cloned.1.call-done = bf16[512,2048]{1,0:T(8,128)(2,1)} async-done(((bf16[16,2048]{1,0:T(8,128)(2,1)}), bf16[512,2048]{1,0:T(8,128)(2,1)}) %all-gather.2.cloned.1.call-update) | async-done | bytes 2097168 | tf_op jit(solution)/shard_map/all_gather | solution.py:152
  78.1 3.5 %fusion.82 = f32[1,512]{1,0:T(1,128)S(1)} fusion(bf16[512,2048]{1,0:T(8,128)(2,1)} %all-gather.2.cloned.1.call-done, f32[2048,1]{0,1:T(1,128)S(1)} %bitcast.65), kind=kOutput, calls=%fused_computation.116 | convolution fusion | flops 12582912 | bytes 2107392 | tf_op jit(solution)/shard_map/dot_general | solution.py:154
  81.6 2.8 %fusion.83 = f32[512,256]{1,0:T(8,128)} fusion(bf16[512,2048]{1,0:T(8,128)(2,1)S(1)} %copy-done.1, bf16[2048,256]{1,0:T(8,128)(2,1)} %param.49), kind=kOutput, calls=%fused_computation.117 | convolution fusion | flops 536870912 | bytes 3670016 | tf_op jit(solution)/shard_map/dot_general | solution.py:156
  84.4 6.2 %fusion.18 = f32[512,2048]{1,0:T(8,128)} fusion(bf16[256,2048]{1,0:T(8,128)(2,1)S(1)} %copy-done.5, bf16[512,2048]{1,0:T(8,128)(2,1)} %all-gather.2.cloned.1.call-done, bf16[2048,256]{1,0:T(8,128)(2,1)} %param.50, f32[512,256]{1,0:T(8,128)} %fusion.83, f32[512]{0:T(512)S(1)} %add_divide_fusion), kind=kOutput, calls=%fused_computation.22 | convolution fusion | flops 1074659328 | bytes 8914944 | tf_op jit(solution)/shard_map/dot_general | solution.py:179
  90.7 0.7 copy-done.15
  91.6 0.1 eq.28
  91.8 0.1 reshape.147
  92.0 0.1 reduce_window_sum.11
  92.1 0.2 select_reduce_fusion.2
  92.3 2.2 scatter_custom_fusion
  94.5 1.5 reshape.129
  96.0 33.8 %all_to_all.10 = bf16[32,7,2048]{2,1,0:T(8,128)(2,1)} all-to-all(bf16[32,7,2048]{2,1,0:T(8,128)(2,1)S(1)} %reshape.129), channel_id=1, replica_groups=mesh['ep'=32] {'ep'}, dimensions={0} | all-to-all | bytes 1835008 | tf_op jit(solution)/shard_map/all_to_all | solution.py:169
  129.8 1.5 reshape.130
  131.3 3.0 %fusion.6 = f32[224,512]{1,0:T(8,128)} fusion(bf16[224,2048]{1,0:T(8,128)(2,1)S(1)} %reshape.130, bf16[1,2048,512]{2,1,0:T(8,128)(2,1)} %param.45), kind=kOutput, calls=%fused_computation.10 | convolution fusion | flops 469762048 | bytes 3473408 | tf_op jit(solution)/shard_map/dot_general | solution.py:93
  134.4 3.8 %convolution_convert_fusion = bf16[224,2048]{1,0:T(8,128)(2,1)} fusion(bf16[1,512,2048]{2,1,0:T(8,128)(2,1)S(1)} %copy-done, bf16[224,2048]{1,0:T(8,128)(2,1)S(1)} %reshape.130, bf16[1,2048,512]{2,1,0:T(8,128)(2,1)} %param.46, f32[224,512]{1,0:T(8,128)} %fusion.6), kind=kOutput, calls=%fused_computation.3 | convolution fusion | flops 940670976 | bytes 6488064 | tf_op jit(solution)/shard_map/dot_general | solution.py:96
  138.2 2.4 reshape.131
  140.5 3.5 %all-to-all-start.1 = ((bf16[32,7,2048]{2,1,0:T(8,128)(2,1)}), bf16[32,7,2048]{2,1,0:T(8,128)(2,1)}, u32[]{:S(2)}, u32[]{:S(2)}) async-start(bf16[32,7,2048]{2,1,0:T(8,128)(2,1)} %reshape.131), calls=%async_computation.2 | async-start | bytes 2097152 | tf_op jit(solution)/shard_map/all_to_all | solution.py:172
  144.1 0.1 fusion.79
  144.2 0.1 copy.63
  144.4 0.1 stack_reshape.6
  144.6 0.1 stack_reshape.7
  144.8 0.1 convolution_exponential_fusion
  145.0 0.1 fusion.24
  145.2 0.2 select_reduce_fusion
  145.5 0.7 pad_maximum_fusion
  146.2 27.9 %all-to-all-done.1 = bf16[32,7,2048]{2,1,0:T(8,128)(2,1)} async-done(((bf16[32,7,2048]{2,1,0:T(8,128)(2,1)}), bf16[32,7,2048]{2,1,0:T(8,128)(2,1)}, u32[]{:S(2)}, u32[]{:S(2)}) %all-to-all-start.1) | async-done | bytes 917536 | tf_op jit(solution)/shard_map/all_to_all | solution.py:172
  174.1 1.5 reshape.132
  175.6 0.8 gather_fusion
  176.5 0.1 reshape.134
  176.6 0.4 multiply_reduce_fusion
  177.0 59.3 %reduce-scatter.2.cloned.1.call-done = f32[16,2048]{1,0:T(8,128)} async-done(((f32[512,2048]{1,0:T(8,128)}), f32[16,2048]{1,0:T(8,128)}) %reduce-scatter.2.cloned.1.call-update) | async-done | bytes 131088 | tf_op jit(solution)/shard_map/reduce_scatter | solution.py:178
  236.2 1.6 add_convert_fusion
  (65 shorter events, 1.1 us)
Async XLA Ops:
  7.2 127.2 %copy-start = (bf16[1,512,2048]{2,1,0:T(8,128)(2,1)S(1)}, bf16[1,512,2048]{2,1,0:T(8,128)(2,1)}, u32[]{:S(2)}) copy-start(bf16[1,512,2048]{2,1,0:T(8,128)(2,1)} %param.47) | copy-start | bytes 6291460
  7.2 4.6 %copy-start.12 = (f32[2,16,2048]{2,1,0:T(8,128)S(1)}, f32[2,16,2048]{2,1,0:T(8,128)}, u32[]{:S(2)}) copy-start(f32[2,16,2048]{2,1,0:T(8,128)} %param.27) | copy-start | bytes 786436
  7.2 5.8 %copy-start.7 = (f32[32,64,16]{1,2,0:T(8,128)S(1)}, f32[32,64,16]{1,2,0:T(8,128)}, u32[]{:S(2)}) copy-start(f32[32,64,16]{1,2,0:T(8,128)} %param.34) | copy-start | bytes 393220
  7.2 5.8 %copy-start.8 = (f32[32,64,16]{1,2,0:T(8,128)S(1)}, f32[32,64,16]{1,2,0:T(8,128)}, u32[]{:S(2)}) copy-start(f32[32,64,16]{1,2,0:T(8,128)} %param.33) | copy-start | bytes 393220
  7.2 70.9 %all-gather.2.cloned.1.call-start = ((), (), s32[]{:S(2)}) async-start(), calls=%async_computation.3 | async-start | bytes 2162688 | tf_op jit(solution)/shard_map/all_gather | solution.py:152
  12.0 2.1 copy-start.11
  12.1 2.7 %copy-start.13 = (f32[32,16,64]{2,1,0:T(8,128)S(1)}, f32[32,16,64]{2,1,0:T(8,128)}, u32[]{:S(2)}) copy-start(f32[32,16,64]{2,1,0:T(8,128)} %param.36) | copy-start | bytes 393220
  13.6 1.1 copy-start.2
  14.1 1.4 copy-start.18
  14.2 1.4 copy-start.10
  14.2 1.6 copy-start.9
  15.3 3.0 %copy-start.17 = (f32[2048]{0:T(1024)S(1)}, f32[2048]{0:T(1024)}, u32[]{:S(2)}) copy-start(f32[2048]{0:T(1024)} %param.41) | copy-start | bytes 24580
  15.4 62.7 %copy-start.16 = (f32[2048]{0:T(1024)S(1)}, f32[2048]{0:T(1024)}, u32[]{:S(2)}) copy-start(f32[2048]{0:T(1024)} %param.48) | copy-start | bytes 24580
  18.2 66.2 %copy-start.4 = (f32[16,2048]{1,0:T(8,128)}, f32[16,2048]{1,0:T(8,128)S(1)}, u32[]{:S(2)}) copy-start(f32[16,2048]{1,0:T(8,128)S(1)} %get-tuple-element.13) | copy-start | bytes 393220
  19.0 217.2 %reduce-scatter.2.cloned.1.call-start = ((), (), s32[]{:S(2)}) async-start(), calls=%async_computation.4 | async-start | bytes 4325376 | tf_op jit(solution)/shard_map/reduce_scatter | solution.py:178
  78.1 3.5 %copy-start.1 = (bf16[512,2048]{1,0:T(8,128)(2,1)S(1)}, bf16[512,2048]{1,0:T(8,128)(2,1)}, u32[]{:S(2)}) copy-start(bf16[512,2048]{1,0:T(8,128)(2,1)} %all-gather.2.cloned.1.call-done) | copy-start | bytes 6291460
  81.5 2.9 %copy-start.5 = (bf16[256,2048]{1,0:T(8,128)(2,1)S(1)}, bf16[256,2048]{1,0:T(8,128)(2,1)}, u32[]{:S(2)}) copy-start(bf16[256,2048]{1,0:T(8,128)(2,1)} %param.51) | copy-start | bytes 3145732
  90.7 0.7 copy-start.15
  90.7 1.0 copy-start.6
  138.2 5.9 %copy-start.19 = (bf16[2048,4]{0,1:T(4,128)(2,1)S(1)}, bf16[2048,4]{0,1:T(4,128)(2,1)}, u32[]{:S(2)}) copy-start(bf16[2048,4]{0,1:T(4,128)(2,1)} %param.42) | copy-start | bytes 49156
  138.2 6.2 %copy-start.3 = (f32[16,32,64]{2,0,1:T(8,128)S(1)}, f32[16,32,64]{2,0,1:T(8,128)}, u32[]{:S(2)}) copy-start(f32[16,32,64]{2,0,1:T(8,128)} %copy-done.2) | copy-start | bytes 393220
  140.5 4.2 %copy-start.14 = (bf16[2048,32]{0,1:T(8,128)(2,1)S(1)}, bf16[2048,32]{0,1:T(8,128)(2,1)}, u32[]{:S(2)}) copy-start(bf16[2048,32]{0,1:T(8,128)(2,1)} %param.43) | copy-start | bytes 393220
  140.5 33.6 %all-to-all-start.1 = ((bf16[32,7,2048]{2,1,0:T(8,128)(2,1)}), bf16[32,7,2048]{2,1,0:T(8,128)(2,1)}, u32[]{:S(2)}, u32[]{:S(2)}) async-start(bf16[32,7,2048]{2,1,0:T(8,128)(2,1)} %reshape.131), calls=%async_computation.2 | async-start | bytes 2097152 | tf_op jit(solution)/shard_map/all_to_all | solution.py:172
Sparse Core Ops, SparseCore 0:
  19.1 58.9 all-gather.1
  90.8 145.3 reduce-scatter.1
where the time goes:
time: 245 us
  waiting for transfers between devices  146 us (60%)
  blocking collectives  33.8 us (14%)
  matrix products  26.5 us (11%)
  between operations  14.5 us (6%)
  local copies, waits for them, and re-layouts  13.9 us (6%)
  other arithmetic  6.15 us (3%)
  starting transfers between devices  3.61 us (1%)
    reduce_scatter x1, waiting for transfers between devices, on_device(): lax.psum_scatter(jnp.dot(hidden_all, dense_down, preferred_element_type=j...  59.3 us
    all_gather x1, waiting for transfers between devices, on_device(): piece = lax.all_gather(normed, 'ep', axis=0, tiled=True)  59 us
    all_to_all x1, blocking collectives, on_device(): lax.all_to_all(outgoing, 'ep', split_axis=0, concat_axis=0, tiled=True)  33.8 us
    all_to_all x1, waiting for transfers between devices, on_device(): lax.all_to_all(result.reshape(senders, items, inner_width), 'ep', split_a...  27.9 us
    dot_general x1, matrix products, on_device(): jnp.dot(hidden_all, dense_down, preferred_element_type=jnp.float32)  6.23 us
  transfers between devices with their start and end apart: 3, of which 3 were waited for; matrix products, arithmetic and copies ran while one was open for 8% of the time, Pallas kernels for 0%

commit v1 on v0

--- a/solution.py
+++ b/solution.py
@@ -1,6 +1,10 @@
+import functools
+
 import jax
 import jax.numpy as jnp
 from jax import lax
+from jax.experimental import pallas as pl
+from jax.experimental.pallas import tpu as pltpu
 from jax.sharding import PartitionSpec as P
 
 EPS = 1e-05
@@ -83,20 +87,197 @@
     inner_prob = inner_exp / jnp.sum(inner_exp, axis=2, keepdims=True)
     joint = (group_prob[:, :, None] * inner_prob).reshape(row_count, expert_count)
     inner_flat = inner_prob.reshape(row_count, expert_count)
-    matched = route_ids[:, :, None] == jnp.arange(expert_count, dtype=jnp.int32)[None, None, :]
-    picked_joint = jnp.sum(jnp.where(matched, joint[:, None, :], 0.0), axis=2)
-    picked_inner = jnp.sum(jnp.where(matched, inner_flat[:, None, :], 0.0), axis=2)
-    return picked_joint / jnp.sum(picked_inner, axis=1, keepdims=True)
-
-
-def expert_rows(rows_in, w_gate, w_up, w_down):
-    gate_part = jnp.dot(rows_in, w_gate, preferred_element_type=jnp.float32)
-    up_part = jnp.dot(rows_in, w_up, preferred_element_type=jnp.float32)
-    hidden = (jax.nn.silu(gate_part) * up_part).astype(jnp.bfloat16)
-    return jnp.dot(hidden, w_down, preferred_element_type=jnp.float32).astype(jnp.bfloat16)
+    matched = jnp.any(
+        route_ids[:, :, None] == jnp.arange(expert_count, dtype=jnp.int32)[None, None, :], axis=1
+    )
+    chosen_inner = jnp.sum(jnp.where(matched, inner_flat, 0.0), axis=1, keepdims=True)
+    return jnp.where(matched, joint / chosen_inner, 0.0)
+
+
+MESH_ID = pl.DeviceIdType.MESH
+
+
+def chip_offsets(chips):
+    far = chips // 4
+    steps = [(f, m, n) for f in range(far) for m in range(2) for n in range(2)]
+    return sorted(steps, key=lambda s: (min(s[0], far - s[0]) + s[1] + s[2], s))[1:]
+
+
+def chip_at(chip, step, chips, sign):
+    far = chips // 4
+    f, m, n = step
+    return (
+        ((chip // 4 + far + sign * f) % far) * 4
+        + ((chip // 2 + m) % 2) * 2
+        + (chip + n) % 2
+    )
+
+
+def meet(partners):
+    barrier = pltpu.get_barrier_semaphore()
+    for partner in partners:
+        pl.semaphore_signal(barrier, inc=1, device_id=(partner,), device_id_type=MESH_ID)
+    pl.semaphore_wait(barrier, len(partners))
+
+
+def remote(src, dst, send_sem, recv_sem, device):
+    return pltpu.make_async_remote_copy(
+        src_ref=src,
+        dst_ref=dst,
+        send_sem=send_sem,
+        recv_sem=recv_sem,
+        device_id=(device,),
+        device_id_type=MESH_ID,
+    )
+
+
+def gather_kernel(chips, own_ref, all_ref, own_sem, send_sem, recv_sem, pass_send, pass_recv):
+    me = lax.axis_index("ep")
+    chip, core = me // 2, me % 2
+    sibling = chip * 2 + 1 - core
+    steps = chip_offsets(chips)
+    targets = [chip_at(chip, step, chips, 1) * 2 + core for step in steps]
+    meet([sibling] + targets)
+    stay = pltpu.make_async_copy(own_ref, all_ref.at[me], own_sem)
+    sends = [
+        remote(own_ref, all_ref.at[me], send_sem.at[i], recv_sem.at[i], target)
+        for i, target in enumerate(targets)
+    ]
+    for send in sends:
+        send.start()
+    passes = [remote(own_ref, all_ref.at[me], pass_send.at[0], pass_recv.at[0], sibling)]
+    passes[0].start()
+    stay.start()
+    for i, step in enumerate(steps):
+        source = chip_at(chip, step, chips, -1) * 2 + core
+        sends[i].wait_recv()
+        onward = remote(
+            all_ref.at[source],
+            all_ref.at[source],
+            pass_send.at[i + 1],
+            pass_recv.at[i + 1],
+            sibling,
+        )
+        onward.start()
+        passes.append(onward)
+    stay.wait()
+    for send in sends:
+        send.wait_send()
+    for onward in passes:
+        onward.wait()
+
+
+def gather_rows(own, n):
+    chips = n // 2
+    rows, width = own.shape
+    return pl.pallas_call(
+        functools.partial(gather_kernel, chips),
+        out_shape=jax.ShapeDtypeStruct((n, rows, width), own.dtype),
+        in_specs=[pl.BlockSpec(memory_space=pltpu.VMEM)],
+        out_specs=pl.BlockSpec(memory_space=pltpu.VMEM),
+        scratch_shapes=[
+            pltpu.SemaphoreType.DMA,
+            pltpu.SemaphoreType.DMA((chips - 1,)),
+            pltpu.SemaphoreType.DMA((chips - 1,)),
+            pltpu.SemaphoreType.DMA((chips,)),
+            pltpu.SemaphoreType.DMA((chips,)),
+        ],
+        compiler_params=pltpu.CompilerParams(collective_id=0, has_side_effects=True),
+        cost_estimate=pl.CostEstimate(flops=0, bytes_accessed=60_000_000, transcendentals=0),
+        name="gather_rows",
+    )(own)
+
+
+def scatter_kernel(
+    chips,
+    terms_ref,
+    resid_ref,
+    out_ref,
+    pair_in,
+    staged,
+    landed,
+    total,
+    pair_send,
+    pair_recv,
+    send_sem,
+    recv_sem,
+):
+    me = lax.axis_index("ep")
+    chip, core = me // 2, me % 2
+    sibling = chip * 2 + 1 - core
+    steps = chip_offsets(chips)[::-1]
+    others = [chip_at(chip, step, chips, 1) for step in steps]
+    meet([sibling] + [other * 2 + core for other in others])
+    pairs = []
+    for i, other in enumerate(others + [chip]):
+        pair = remote(
+            terms_ref.at[other * 2 + 1 - core],
+            pair_in.at[i],
+            pair_send.at[i],
+            pair_recv.at[i],
+            sibling,
+        )
+        pair.start()
+        pairs.append(pair)
+    sends = []
+    for i, other in enumerate(others):
+        pairs[i].wait_recv()
+        mine = terms_ref[other * 2 + core].astype(jnp.float32)
+        staged[i] = (mine + pair_in[i].astype(jnp.float32)).astype(staged.dtype)
+        sends.append(
+            remote(staged.at[i], landed.at[i], send_sem.at[i], recv_sem.at[i], other * 2 + core)
+        )
+        if i:
+            sends[i - 1].start()
+    last = len(others)
+    pairs[last].wait_recv()
+    total[...] = (
+        resid_ref[...].astype(jnp.float32)
+        + terms_ref[me].astype(jnp.float32)
+        + pair_in[last].astype(jnp.float32)
+    )
+    sends[-1].start()
+    for i in range(len(others))[::-1]:
+        sends[i].wait_recv()
+        total[...] += landed[i].astype(jnp.float32)
+    out_ref[...] = total[...].astype(out_ref.dtype)
+    for send in sends:
+        send.wait_send()
+    for pair in pairs:
+        pair.wait_send()
+
+
+def scatter_rows(terms, resid):
+    n, rows, width = terms.shape
+    chips = n // 2
+    return pl.pallas_call(
+        functools.partial(scatter_kernel, chips),
+        out_shape=jax.ShapeDtypeStruct(resid.shape, resid.dtype),
+        in_specs=[pl.BlockSpec(memory_space=pltpu.VMEM)] * 2,
+        out_specs=pl.BlockSpec(memory_space=pltpu.VMEM),
+        scratch_shapes=[
+            pltpu.VMEM((chips, rows, width), terms.dtype),
+            pltpu.VMEM((chips - 1, rows, width), terms.dtype),
+            pltpu.VMEM((chips - 1, rows, width), terms.dtype),
+            pltpu.VMEM((rows, width), jnp.float32),
+            pltpu.SemaphoreType.DMA((chips,)),
+            pltpu.SemaphoreType.DMA((chips,)),
+            pltpu.SemaphoreType.DMA((chips - 1,)),
+            pltpu.SemaphoreType.DMA((chips - 1,)),
+        ],
+        compiler_params=pltpu.CompilerParams(collective_id=1, has_side_effects=True),
+        name="scatter_rows",
+    )(terms, resid)
+
+
+def in_pieces(values):
+    high = lax.reduce_precision(values, 8, 7)
+    middle = lax.reduce_precision(values - high, 8, 7)
+    return jnp.concatenate([high, middle, values - high - middle], axis=1).astype(jnp.bfloat16)
 
 
 def on_device(
+    n,
     tokens,
     state,
     norm_mix,
@@ -142,46 +323,35 @@
         w_output,
     )
     normed = rms_scale(resid, norm_ffn)
-    seq_count, width = normed.shape
-    topk = route_ids.shape[1]
     expert_count = w_expert.shape[1]
-    capacity = max(2, 5 * seq_count * topk // (2 * expert_count))
-    own_gate = expert_gate[0]
-    own_up = expert_up[0]
-    own_down = expert_down[0]
-    piece = lax.all_gather(normed, "ep", axis=0, tiled=True)
+    rows, width = normed.shape
+    gates = route_gates(normed, w_group, w_expert, route_ids)
     branch_gate = jax.nn.sigmoid(
-        jnp.dot(piece.astype(jnp.float32), dense_vector, precision=HIGH_PRECISION)
-    )
-    dense_g = jnp.dot(piece, dense_gate, preferred_element_type=jnp.float32)
-    dense_u = jnp.dot(piece, dense_up, preferred_element_type=jnp.float32)
-    hidden_all = (branch_gate[:, None] * jax.nn.silu(dense_g) * dense_u).astype(jnp.bfloat16)
-    gates = route_gates(normed, w_group, w_expert, route_ids)
-    flat_ids = route_ids.reshape(-1)
-    onehot = (flat_ids[:, None] == jnp.arange(expert_count, dtype=jnp.int32)[None, :]).astype(
-        jnp.int32
-    )
-    ordinal = jnp.sum((jnp.cumsum(onehot, axis=0) - 1) * onehot, axis=1)
-    target = flat_ids * capacity + ordinal
-    source_rows = jnp.repeat(normed, topk, axis=0)
-    outgoing = jnp.zeros((expert_count * capacity, width), jnp.bfloat16).at[target].set(source_rows)
-    outgoing = outgoing.reshape(expert_count, capacity, width)
-    received = lax.all_to_all(outgoing, "ep", split_axis=0, concat_axis=0, tiled=True)
-    senders, items, inner_width = received.shape
-    result = expert_rows(received.reshape(senders * items, inner_width), own_gate, own_up, own_down)
-    returned = lax.all_to_all(
-        result.reshape(senders, items, inner_width), "ep", split_axis=0, concat_axis=0, tiled=True
-    )
-    picked = returned.reshape(expert_count * capacity, width)[target]
-    weighted = picked.astype(jnp.float32).reshape(seq_count, topk, width) * gates[:, :, None]
-    local_moe = jnp.sum(weighted, axis=1)
-    summed = lax.psum_scatter(
-        jnp.dot(hidden_all, dense_down, preferred_element_type=jnp.float32),
-        "ep",
-        scatter_dimension=0,
-        tiled=True,
-    )
-    layer_out = (resid.astype(jnp.float32) + summed + local_moe).astype(jnp.bfloat16)
+        jnp.dot(normed.astype(jnp.float32), dense_vector, precision=HIGH_PRECISION)
+    )
+    scales = in_pieces(jnp.concatenate([gates, branch_gate[:, None]], axis=1))
+    scales = jnp.pad(scales, ((0, 0), (0, -scales.shape[1] % 128)))
+    gathered = gather_rows(jnp.concatenate([normed, scales], axis=1), n)
+    gathered = gathered.reshape(n * rows, -1)
+    piece, scales = gathered[:, :width], gathered[:, width:].astype(jnp.float32)
+    stride = expert_count + 1
+    column = jnp.arange(scales.shape[1], dtype=jnp.int32)
+    owner = jnp.where(column < 3 * stride, column % stride, stride)
+    me = lax.axis_index("ep")
+    own_weight = jnp.sum(jnp.where(owner == me, scales, 0.0), axis=1, keepdims=True)
+    branch_all = jnp.sum(jnp.where(owner == expert_count, scales, 0.0), axis=1, keepdims=True)
+
+    def hidden_units(w_gate, w_up, scale):
+        gate_part = jnp.dot(piece, w_gate, preferred_element_type=jnp.float32)
+        up_part = jnp.dot(piece, w_up, preferred_element_type=jnp.float32)
+        return (scale * jax.nn.silu(gate_part) * up_part).astype(jnp.bfloat16)
+
+    dense_hidden = hidden_units(dense_gate, dense_up, branch_all)
+    expert_hidden = hidden_units(expert_gate[0], expert_up[0], own_weight)
+    terms = jnp.dot(dense_hidden, dense_down, preferred_element_type=jnp.float32) + jnp.dot(
+        expert_hidden, expert_down[0], preferred_element_type=jnp.float32
+    )
+    layer_out = scatter_rows(terms.astype(jnp.bfloat16).reshape(n, rows, width), resid)
     return (layer_out, new_state)
 
 
@@ -215,7 +385,7 @@
         P("ep", None),
     )
     return jax.shard_map(
-        on_device,
+        functools.partial(on_device, mesh.shape["ep"]),
         mesh=mesh,
         in_specs=placed,
         out_specs=(P("ep", None), P(None, "ep", None)),

time: 245 us -> 111 us (0.45)
  waiting for transfers between devices: 146 us -> 0 us
  Pallas kernels: 0 us -> 66.7 us
  blocking collectives: 33.8 us -> 0 us
  between operations: 14.5 us -> 1.02 us
  local copies, waits for them, and re-layouts: 13.9 us -> 4.38 us
  matrix products: 26.5 us -> 30.6 us
  starting transfers between devices: 3.61 us -> 0 us
    pallas_call x0 -> x2, Pallas kernels: none -> 66.7 us  [the longest x1 35.6 us: gather_rows(): pl.pallas_call(functools.partial(gather_kernel, chips), out_shape=jax.Sha...]
    reduce_scatter x1 -> x0, waiting for transfers between devices: 59.3 us -> none  [on_device(): lax.psum_scatter(jnp.dot(hidden_all, dense_down, preferred_element_type=j...]
    all_gather x1 -> x0, waiting for transfers between devices: 59 us -> none  [on_device(): piece = lax.all_gather(normed, 'ep', axis=0, tiled=True)]
    all_to_all x1 -> x0, blocking collectives: 33.8 us -> none  [on_device(): lax.all_to_all(outgoing, 'ep', split_axis=0, concat_axis=0, tiled=True)]
    all_to_all x1 -> x0, waiting for transfers between devices: 27.9 us -> none  [on_device(): lax.all_to_all(result.reshape(senders, items, inner_width), 'ep', split_a...]
    reshape x5 -> x0, local copies, waits for them, and re-layouts: 6.95 us -> none  [the longest x1 2.36 us: on_device(): result.reshape(senders, items, inner_width)]
    all_to_all x1 -> x0, starting transfers between devices: 3.53 us -> none  [on_device(): lax.all_to_all(result.reshape(senders, items, inner_width), 'ep', split_a...]
  transfers between devices with their start and end apart: 3 -> 0, of which waited for: 3 -> 0; matrix products, arithmetic and copies ran while one was open for 8% -> 0% of each run, Pallas kernels for 0% -> 0%
where the time goes in v1:
time: 111 us; the launch traced here: 110 us
  Pallas kernels  66.7 us (60%)
  matrix products  30.6 us (28%)
  other arithmetic  7.63 us (7%)
  local copies, waits for them, and re-layouts  4.38 us (4%)
    pallas_call x1, Pallas kernels, gather_rows(): pl.pallas_call(functools.partial(gather_kernel, chips), out_shape=jax.Sha...  35.6 us
    pallas_call x1, Pallas kernels, scatter_rows(): pl.pallas_call(functools.partial(scatter_kernel, chips), out_shape=jax.Sh...  31.1 us
    dot_general x1, matrix products, on_device(): jnp.dot(expert_hidden, expert_down[0], preferred_element_type=jnp.float32)  7.56 us
    dot_general x1, matrix products, on_device(): jnp.dot(dense_hidden, dense_down, preferred_element_type=jnp.float32)  6.23 us
    dot_general x2, matrix products, hidden_units(): gate_part = jnp.dot(piece, w_gate, preferred_element_type=jnp.float32)  5.84 us
    dot_general x1, matrix products, state_mixer(): jnp.dot(mixed, w_output, preferred_element_type=jnp.float32)  2.44 us

profile of v1, /device:TPU:0, one launch (start us, length us, event | category | flops | bytes accessed | tf_op | source)
XLA Modules:
  0.0 110.4 jit_solution(12236384866239321773)
XLA Ops:
  0.6 0.0 copy-start
  0.7 0.0 copy-start.4
  0.7 0.8 exp.26
  1.5 1.0 fusion.69
  2.5 0.6 broadcast_compare_fusion
  3.1 1.4 %fusion.81 = pred[16,32]{1,0:T(8,128)(4,1)} fusion(s32[16,6]{0,1:T(8,128)} %param.44), kind=kLoop, calls=%fused_computation.84 | loop fusion | flops 5632 | bytes 896 | tf_op jit(solution)/shard_map/reduce_or | solution.py:90
  4.5 2.1 %convolution_convert_fusion = bf16[16,512]{1,0:T(8,128)(2,1)S(1)} fusion(bf16[2048,512]{1,0:T(8,128)(2,1)} %param.29, bf16[16,2048]{1,0:T(8,128)(2,1)} %param.26, f32[2048]{0:T(1024)} %param.28, f32[16]{0:T(128)S(1)} %add_rsqrt_fusion.1), kind=kOutput, calls=%fused_computation.31 | convolution fusion | flops 33693696 | bytes 2187328 | tf_op jit(solution)/shard_map/dot_general | solution.py:41
  6.5 0.0 copy-done.14
  6.6 0.8 cosine_multiply_fusion
  7.3 0.1 reshape.55
  7.5 0.1 reshape_squeeze.6
  7.6 0.1 reshape_squeeze.7
  7.8 1.3 %fusion.28 = f32[16,32,64]{2,0,1:T(8,128)S(1)} fusion(f32[32,64,16]{1,2,0:T(8,128)S(1)} %copy-done.4, f32[32,64,16]{1,2,0:T(8,128)S(1)} %copy-done.3, f32[16,32,64]{2,1,0:T(8,128)S(1)} %reshape_squeeze.7, f32[16,32,64]{2,1,0:T(8,128)S(1)} %reshape_squeeze.6, f32[32,64]{1,0:T(8,128)} %get-tuple-element.8, f32[32,64]{1,0:T(8,128)} %get-tuple-element.9, ...), kind=kOutput, calls=%fused_computation.22 | convolution fusion | flops 6520832 | bytes 704512 | tf_op jit(solution)/shard_map/gpc,sgc->sgp/dot_general | solution.py:54
  9.0 1.5 %fusion.29 = f32[16,32,64]{2,0,1:T(8,128)S(1)} fusion(f32[32,64,16]{1,2,0:T(8,128)S(1)} %copy-done.3, f32[32,64,16]{1,2,0:T(8,128)} %param.33, f32[16,32,64]{2,1,0:T(8,128)S(1)} %reshape_squeeze.7, f32[16,32,64]{2,1,0:T(8,128)S(1)} %reshape_squeeze.6, f32[32,64]{1,0:T(8,128)} %get-tuple-element.8, f32[32,64]{1,0:T(8,128)} %get-tuple-element.9, ...), kind=kOutput, calls=%fused_computation.24 | convolution fusion | flops 6520832 | bytes 704512 | tf_op jit(solution)/shard_map/gpc,sgc->sgp/dot_general | solution.py:53
  10.5 0.1 copy.59
  10.6 0.8 stack_reshape.6
  11.4 1.5 %fusion.104 = f32[32,16,16]{2,1,0:T(8,128)S(1)} fusion(f32[16,32,64]{2,0,1:T(8,128)S(1)} %fusion.29, f32[32,16,64]{2,1,0:T(8,128)} %param.35), kind=kOutput, calls=%fused_computation.130 | convolution fusion | flops 6291456 | bytes 294912 | tf_op jit(solution)/shard_map/xej,fxj->fxe/dot_general | solution.py:59
  13.0 1.5 %fusion.27 = f32[16,32,16]{2,0,1:T(8,128)S(1)} fusion(f32[32,16,16]{2,1,0:T(8,128)S(1)} %fusion.104, f32[16,32,64]{2,0,1:T(8,128)S(1)} %fusion.28, f32[32,16,64]{2,1,0:T(8,128)} %param.36), kind=kOutput, calls=%fused_computation.20 | convolution fusion | flops 6299648 | bytes 327680 | tf_op jit(solution)/shard_map/xej,fxj->fxe/dot_general | solution.py:61
  14.5 0.1 copy.60
  14.6 0.1 stack_reshape.7
  14.7 1.6 %pad_maximum_fusion = f32[2,16,2048]{2,1,0:T(8,128)} fusion(f32[1,16,2048]{2,1,0:T(8,128)S(1)} %stack_reshape.7, f32[1,16,2048]{2,1,0:T(8,128)} %stack_reshape.6), kind=kLoop, calls=%fused_computation.54 | loop fusion | flops 65536 | bytes 524288 | tf_op jit(solution)/shard_map/stack | solution.py:71
  16.3 0.1 copy.54
  16.4 0.2 reshape.56
  16.7 0.2 fusion.105
  16.8 2.4 %fusion.66 = (f32[16]{0:T(128)S(1)}, bf16[16,2048]{1,0:T(8,128)(2,1)S(1)}) fusion(bf16[512,2048]{1,0:T(8,128)(2,1)} %param.40, f32[16,512]{1,0:T(8,128)S(1)} %fusion.105, bf16[16,512]{1,0:T(8,128)(2,1)S(1)} %fusion.89, bf16[512,512]{1,0:T(8,128)(2,1)} %param.39, bf16[16,2048]{1,0:T(8,128)(2,1)S(1)} %copy-done.5), kind=kOutput, calls=%fused_computation.67 | convolution fusion | flops 42180592 | bytes 2801728 | tf_op jit(solution)/shard_map/dot_general | solution.py:69
  19.3 0.1 fusion.68
  19.4 0.1 fusion.43
  19.6 0.0 copy-done.20
  19.6 0.2 fusion.103
  19.8 0.1 copy.58
  19.9 0.2 convolution_exponential_fusion
  20.0 0.1 copy.57
  20.1 0.1 copy.55
  20.2 0.1 fusion.38
  20.3 0.1 copy.56
  20.4 0.1 select_reduce_fusion
  20.5 0.1 divide_select_fusion
  20.6 0.1 reduce-precision_convert_fusion.1
  20.7 0.1 fusion.98
  20.7 0.6 pad_maximum_fusion.1.own_ref
  21.4 35.6 %gather_rows.1 = bf16[32,16,2176]{2,1,0:T(8,128)(2,1)} custom-call(bf16[16,2176]{1,0:T(8,128)(2,1)} %pad_maximum_fusion.1.own_ref), custom_call_target="tpu_custom_call" | custom-call | bytes 60000000 | tf_op jit(solution)/shard_map/gather_rows/pallas_call | solution.py:173
  57.0 1.1 fusion.57
  58.1 3.5 %fusion.14 = f32[512,256]{1,0:T(8,128)} fusion(bf16[2048,256]{1,0:T(8,128)(2,1)} %param.49, bf16[512,2176]{1,0:T(8,128)(2,1)} %bitcast.70), kind=kOutput, calls=%fused_computation.14 | convolution fusion | flops 536870912 | bytes 3670016 | tf_op jit(solution)/shard_map/dot_general | solution.py:345
  61.7 2.3 %fusion.5 = f32[512,512]{1,0:T(8,128)} fusion(bf16[1,2048,512]{2,1,0:T(8,128)(2,1)S(1)} %copy-done.19, bf16[512,2176]{1,0:T(8,128)(2,1)S(1)} %bitcast.73), kind=kOutput, calls=%fused_computation.7 | convolution fusion | flops 1073741824 | bytes 5242880 | tf_op jit(solution)/shard_map/dot_general | solution.py:345
  64.0 6.2 %fusion.31 = f32[512,2048]{1,0:T(8,128)} fusion(bf16[256,2048]{1,0:T(8,128)(2,1)S(1)} %copy-done.2, bf16[2048,256]{1,0:T(8,128)(2,1)} %param.50, bf16[512,2176]{1,0:T(8,128)(2,1)} %bitcast.71, f32[512,256]{1,0:T(8,128)} %fusion.14, f32[512]{0:T(512)S(1)} %get-tuple-element.3), kind=kOutput, calls=%fused_computation.25 | convolution fusion | flops 1074659328 | bytes 8914944 | tf_op jit(solution)/shard_map/dot_general | solution.py:351
  70.2 7.6 %add_convert_fusion = bf16[512,2048]{1,0:T(8,128)(2,1)} fusion(f32[512,2048]{1,0:T(8,128)} %fusion.31, bf16[1,512,2048]{2,1,0:T(8,128)(2,1)S(1)} %copy-done, bf16[1,2048,512]{2,1,0:T(8,128)(2,1)} %param.46, bf16[512,2176]{1,0:T(8,128)(2,1)} %bitcast.72, f32[512,512]{1,0:T(8,128)} %fusion.5, f32[512]{0:T(512)S(1)} %get-tuple-element.2), kind=kOutput, calls=%fused_computation.1 | convolution fusion | flops 2151415808 | bytes 13633536 | tf_op jit(solution)/shard_map/dot_general | solution.py:351
  77.8 31.1 %scatter_rows.1 = bf16[16,2048]{1,0:T(8,128)(2,1)} custom-call(bf16[32,16,2048]{2,1,0:T(8,128)(2,1)} %bitcast.74, bf16[16,2048]{1,0:T(8,128)(2,1)} %copy-done.6), custom_call_target="tpu_custom_call" | custom-call | tf_op jit(solution)/shard_map/scatter_rows/pallas_call | solution.py:253
  108.9 1.5 %copy.70 = bf16[16,2048]{1,0:T(8,128)(2,1)} copy(bf16[16,2048]{1,0:T(8,128)(2,1)} %scatter_rows.1) | data formatting | bytes 131072
  (46 shorter events, 0.2 us)
Async XLA Ops:
  0.6 69.6 %copy-start = (bf16[1,512,2048]{2,1,0:T(8,128)(2,1)S(1)}, bf16[1,512,2048]{2,1,0:T(8,128)(2,1)}, u32[]{:S(2)}) copy-start(bf16[1,512,2048]{2,1,0:T(8,128)(2,1)} %param.47) | copy-start | bytes 6291460
  0.6 7.1 %copy-start.3 = (f32[32,64,16]{1,2,0:T(8,128)S(1)}, f32[32,64,16]{1,2,0:T(8,128)}, u32[]{:S(2)}) copy-start(f32[32,64,16]{1,2,0:T(8,128)} %param.34) | copy-start | bytes 393220
  0.7 7.1 %copy-start.4 = (f32[32,64,16]{1,2,0:T(8,128)S(1)}, f32[32,64,16]{1,2,0:T(8,128)}, u32[]{:S(2)}) copy-start(f32[32,64,16]{1,2,0:T(8,128)} %param.33) | copy-start | bytes 393220
  0.7 5.9 %copy-start.13 = (f32[32,64]{1,0:T(8,128)S(1)}, f32[32,64]{1,0:T(8,128)}, u32[]{:S(2)}) copy-start(f32[32,64]{1,0:T(8,128)} %param.31) | copy-start | bytes 24580
  0.7 5.9 %copy-start.14 = (f32[32,64]{1,0:T(8,128)S(1)}, f32[32,64]{1,0:T(8,128)}, u32[]{:S(2)}) copy-start(f32[32,64]{1,0:T(8,128)} %param.30) | copy-start | bytes 24580
  0.7 6.8 %copy-start.8 = (f32[2,16,2048]{2,1,0:T(8,128)S(1)}, f32[2,16,2048]{2,1,0:T(8,128)}, u32[]{:S(2)}) copy-start(f32[2,16,2048]{2,1,0:T(8,128)} %param.27) | copy-start | bytes 786436
  6.6 0.8 copy-start.9
  11.4 5.2 %copy-start.10 = (bf16[16,512]{1,0:T(8,128)(2,1)S(1)}, bf16[16,512]{1,0:T(8,128)(2,1)}, u32[]{:S(2)}) copy-start(bf16[16,512]{1,0:T(8,128)(2,1)} %copy-done.9) | copy-start | bytes 49156
  11.4 5.2 %copy-start.16 = (f32[512]{0:T(512)S(1)}, f32[512]{0:T(512)}, u32[]{:S(2)}) copy-start(f32[512]{0:T(512)} %param.37) | copy-start | bytes 6148
  11.4 5.3 %copy-start.7 = (bf16[512,512]{1,0:T(8,128)(2,1)S(1)}, bf16[512,512]{1,0:T(8,128)(2,1)}, u32[]{:S(2)}) copy-start(bf16[512,512]{1,0:T(8,128)(2,1)} %param.38) | copy-start | bytes 1572868
  13.0 3.9 %copy-start.5 = (bf16[16,2048]{1,0:T(8,128)(2,1)S(1)}, bf16[16,2048]{1,0:T(8,128)(2,1)}, u32[]{:S(2)}) copy-start(bf16[16,2048]{1,0:T(8,128)(2,1)} %param.26) | copy-start | bytes 196612
  16.3 3.0 %copy-start.15 = (f32[2048]{0:T(1024)S(1)}, f32[2048]{0:T(1024)}, u32[]{:S(2)}) copy-start(f32[2048]{0:T(1024)} %param.41) | copy-start | bytes 24580
  16.3 3.1 %copy-start.21 = (f32[2048]{0:T(1024)S(1)}, f32[2048]{0:T(1024)}, u32[]{:S(2)}) copy-start(f32[2048]{0:T(1024)} %param.48) | copy-start | bytes 24580
  16.4 3.2 %copy-start.20 = (bf16[2048,4]{0,1:T(4,128)(2,1)S(1)}, bf16[2048,4]{0,1:T(4,128)(2,1)}, u32[]{:S(2)}) copy-start(bf16[2048,4]{0,1:T(4,128)(2,1)} %param.42) | copy-start | bytes 49156
  16.4 3.5 %copy-start.11 = (bf16[2048,32]{0,1:T(8,128)(2,1)S(1)}, bf16[2048,32]{0,1:T(8,128)(2,1)}, u32[]{:S(2)}) copy-start(bf16[2048,32]{0,1:T(8,128)(2,1)} %param.43) | copy-start | bytes 393220
  16.6 3.8 %copy-start.12 = (pred[16,32]{1,0:T(8,128)(4,1)S(1)}, pred[16,32]{1,0:T(8,128)(4,1)}, u32[]{:S(2)}) copy-start(pred[16,32]{1,0:T(8,128)(4,1)} %fusion.81) | copy-start | bytes 1540
  19.3 42.3 %copy-start.6 = (bf16[16,2048]{1,0:T(8,128)(2,1)}, bf16[16,2048]{1,0:T(8,128)(2,1)S(1)}, u32[]{:S(2)}) copy-start(bf16[16,2048]{1,0:T(8,128)(2,1)S(1)} %get-tuple-element.14.resid_ref) | copy-start | bytes 196612
  19.3 37.7 %copy-start.17 = (pred[128]{0:T(512)(128)(4,1)S(1)}, pred[128]{0:T(512)(128)(4,1)}, u32[]{:S(2)}) copy-start(pred[128]{0:T(512)(128)(4,1)} %get-tuple-element.17) | copy-start | bytes 388
  19.3 37.7 %copy-start.18 = (pred[128]{0:T(512)(128)(4,1)S(1)}, pred[128]{0:T(512)(128)(4,1)}, u32[]{:S(2)}) copy-start(pred[128]{0:T(512)(128)(4,1)} %get-tuple-element.18) | copy-start | bytes 388
  58.1 3.5 %copy-start.1 = (bf16[32,16,2176]{2,1,0:T(8,128)(2,1)S(1)}, bf16[32,16,2176]{2,1,0:T(8,128)(2,1)}, u32[]{:S(2)}) copy-start(bf16[32,16,2176]{2,1,0:T(8,128)(2,1)} %gather_rows.1) | copy-start | bytes 6684676
  58.1 3.5 %copy-start.19 = (bf16[1,2048,512]{2,1,0:T(8,128)(2,1)S(1)}, bf16[1,2048,512]{2,1,0:T(8,128)(2,1)}, u32[]{:S(2)}) copy-start(bf16[1,2048,512]{2,1,0:T(8,128)(2,1)} %param.45) | copy-start | bytes 6291460
  61.6 2.3 %copy-start.2 = (bf16[256,2048]{1,0:T(8,128)(2,1)S(1)}, bf16[256,2048]{1,0:T(8,128)(2,1)}, u32[]{:S(2)}) copy-start(bf16[256,2048]{1,0:T(8,128)(2,1)} %param.51) | copy-start | bytes 3145732

commit v2 on v1

--- a/solution.py
+++ b/solution.py
@@ -97,20 +97,29 @@
 MESH_ID = pl.DeviceIdType.MESH
 
 
-def chip_offsets(chips):
-    far = chips // 4
-    steps = [(f, m, n) for f in range(far) for m in range(2) for n in range(2)]
-    return sorted(steps, key=lambda s: (min(s[0], far - s[0]) + s[1] + s[2], s))[1:]
-
-
-def chip_at(chip, step, chips, sign):
-    far = chips // 4
-    f, m, n = step
-    return (
-        ((chip // 4 + far + sign * f) % far) * 4
-        + ((chip // 2 + m) % 2) * 2
-        + (chip + n) % 2
-    )
+class Place:
+    def __init__(self, chips):
+        me = lax.axis_index("ep")
+        chip, core = me // 2, me % 2
+        near, middle = 1 - 2 * (chip % 2), 2 - 4 * ((chip // 2) % 2)
+        self.me, self.chip, self.core = me, chip, core
+        self.far, self.line = chips // 4, chip // 4
+        self.sibling = chip * 2 + 1 - core
+        first = chip + (1 - core) * near + core * middle
+        second = chip + core * near + (1 - core) * middle
+        self.first, self.second = first * 2 + core, second * 2 + core
+        self.own_row, self.first_row, self.second_row = chip % 4, first % 4, second % 4
+        self.across_row = 3 - self.own_row
+
+    def chip_of(self, step, row):
+        return ((self.line + self.far + step) % self.far) * 4 + row
+
+    def block(self, step, row):
+        return self.chip_of(step, row) * 2 + self.core
+
+    def partners(self):
+        line = [self.block(step, self.own_row) for step in range(1, self.far)]
+        return [self.sibling, self.first, self.second] + line
 
 
 def meet(partners):
@@ -131,40 +140,77 @@
     )
 
 
-def gather_kernel(chips, own_ref, all_ref, own_sem, send_sem, recv_sem, pass_send, pass_recv):
-    me = lax.axis_index("ep")
-    chip, core = me // 2, me % 2
-    sibling = chip * 2 + 1 - core
-    steps = chip_offsets(chips)
-    targets = [chip_at(chip, step, chips, 1) * 2 + core for step in steps]
-    meet([sibling] + targets)
-    stay = pltpu.make_async_copy(own_ref, all_ref.at[me], own_sem)
-    sends = [
-        remote(own_ref, all_ref.at[me], send_sem.at[i], recv_sem.at[i], target)
-        for i, target in enumerate(targets)
+def gather_kernel(
+    chips,
+    own_ref,
+    all_ref,
+    own_sem,
+    line_send,
+    line_recv,
+    first_send,
+    first_recv,
+    second_send,
+    second_recv,
+    pass_send,
+    pass_recv,
+):
+    at = Place(chips)
+    far = at.far
+    meet(at.partners())
+    started = []
+
+    def send(block, send_sem, recv_sem, slot, device):
+        source = own_ref if block is None else all_ref.at[block]
+        target = all_ref.at[at.me if block is None else block]
+        copy = remote(source, target, send_sem.at[slot], recv_sem.at[slot], device)
+        copy.start()
+        started.append(copy)
+        return copy
+
+    lines = [
+        send(None, line_send, line_recv, step - 1, at.block(step, at.own_row))
+        for step in range(1, far)
     ]
-    for send in sends:
-        send.start()
-    passes = [remote(own_ref, all_ref.at[me], pass_send.at[0], pass_recv.at[0], sibling)]
-    passes[0].start()
-    stay.start()
-    for i, step in enumerate(steps):
-        source = chip_at(chip, step, chips, -1) * 2 + core
-        sends[i].wait_recv()
-        onward = remote(
-            all_ref.at[source],
-            all_ref.at[source],
-            pass_send.at[i + 1],
-            pass_recv.at[i + 1],
-            sibling,
-        )
-        onward.start()
-        passes.append(onward)
+    firsts, seconds, passes = [], [], []
+    stay = pltpu.make_async_copy(own_ref, all_ref.at[at.me], own_sem)
+    for step in range(far + 1):
+        if step < far:
+            if step:
+                lines[step - 1].wait_recv()
+            block = at.block(-step, at.own_row) if step else None
+            firsts.append(send(block, first_send, first_recv, step, at.first))
+            seconds.append(send(block, second_send, second_recv, step, at.second))
+            passes.append(send(block, pass_send, pass_recv, step, at.sibling))
+            if step == 0:
+                stay.start()
+        if step:
+            firsts[step - 1].wait_recv()
+            block = at.block(1 - step, at.first_row)
+            slot = far + step - 1
+            seconds.append(send(block, second_send, second_recv, slot, at.second))
+            passes.append(send(block, pass_send, pass_recv, slot, at.sibling))
+    arriving = [(step, at.second_row) for step in range(far)]
+    arriving += [(step, at.across_row) for step in range(far)]
+    by_slot = {}
+    order = list(range(far)) + [far + step for step in range(far)]
+    sent_order = []
+    for step in range(far + 1):
+        if step < far:
+            sent_order.append(step)
+        if step:
+            sent_order.append(far + step - 1)
+    for slot, copy in zip(sent_order, seconds):
+        by_slot[slot] = copy
+    for slot in order:
+        step, row = arriving[slot]
+        by_slot[slot].wait_recv()
+        block = at.block(-step, row)
+        passes.append(send(block, pass_send, pass_recv, 2 * far + slot, at.sibling))
     stay.wait()
-    for send in sends:
-        send.wait_send()
-    for onward in passes:
-        onward.wait()
+    for copy in passes:
+        copy.wait_recv()
+    for copy in started:
+        copy.wait_send()
 
 
 def gather_rows(own, n):
@@ -177,8 +223,12 @@
         out_specs=pl.BlockSpec(memory_space=pltpu.VMEM),
         scratch_shapes=[
             pltpu.SemaphoreType.DMA,
-            pltpu.SemaphoreType.DMA((chips - 1,)),
-            pltpu.SemaphoreType.DMA((chips - 1,)),
+            pltpu.SemaphoreType.DMA((chips // 4 - 1,)),
+            pltpu.SemaphoreType.DMA((chips // 4 - 1,)),
+            pltpu.SemaphoreType.DMA((chips // 4,)),
+            pltpu.SemaphoreType.DMA((chips // 4,)),
+            pltpu.SemaphoreType.DMA((chips // 2,)),
+            pltpu.SemaphoreType.DMA((chips // 2,)),
             pltpu.SemaphoreType.DMA((chips,)),
             pltpu.SemaphoreType.DMA((chips,)),
         ],
@@ -202,47 +252,72 @@
     send_sem,
     recv_sem,
 ):
-    me = lax.axis_index("ep")
-    chip, core = me // 2, me % 2
-    sibling = chip * 2 + 1 - core
-    steps = chip_offsets(chips)[::-1]
-    others = [chip_at(chip, step, chips, 1) for step in steps]
-    meet([sibling] + [other * 2 + core for other in others])
+    at = Place(chips)
+    far = at.far
+    meet(at.partners())
     pairs = []
-    for i, other in enumerate(others + [chip]):
-        pair = remote(
-            terms_ref.at[other * 2 + 1 - core],
-            pair_in.at[i],
-            pair_send.at[i],
-            pair_recv.at[i],
-            sibling,
+    for row in (at.across_row, at.first_row, at.second_row, at.own_row):
+        for step in list(range(1, far)) + [0]:
+            chip = at.chip_of(step, row)
+            pair = remote(
+                terms_ref.at[chip * 2 + 1 - at.core],
+                pair_in.at[chip],
+                pair_send.at[chip],
+                pair_recv.at[chip],
+                at.sibling,
+            )
+            pair.start()
+            pairs.append(pair)
+    sends, waiting = {}, []
+
+    def own_sum(step, row, slots):
+        chip = at.chip_of(step, row)
+        remote(
+            terms_ref.at[chip * 2 + 1 - at.core],
+            pair_in.at[chip],
+            pair_send.at[chip],
+            pair_recv.at[chip],
+            at.sibling,
+        ).wait_recv()
+        value = terms_ref[chip * 2 + at.core].astype(jnp.float32)
+        value = value + pair_in[chip].astype(jnp.float32)
+        for slot in slots:
+            sends[slot].wait_recv()
+            value = value + landed[slot].astype(jnp.float32)
+        return value
+
+    def flush():
+        while waiting:
+            waiting.pop().start()
+
+    def send(slot, value, device):
+        staged[slot] = value.astype(staged.dtype)
+        sends[slot] = remote(
+            staged.at[slot], landed.at[slot], send_sem.at[slot], recv_sem.at[slot], device
         )
-        pair.start()
-        pairs.append(pair)
-    sends = []
-    for i, other in enumerate(others):
-        pairs[i].wait_recv()
-        mine = terms_ref[other * 2 + core].astype(jnp.float32)
-        staged[i] = (mine + pair_in[i].astype(jnp.float32)).astype(staged.dtype)
-        sends.append(
-            remote(staged.at[i], landed.at[i], send_sem.at[i], recv_sem.at[i], other * 2 + core)
-        )
-        if i:
-            sends[i - 1].start()
-    last = len(others)
-    pairs[last].wait_recv()
-    total[...] = (
-        resid_ref[...].astype(jnp.float32)
-        + terms_ref[me].astype(jnp.float32)
-        + pair_in[last].astype(jnp.float32)
-    )
-    sends[-1].start()
-    for i in range(len(others))[::-1]:
-        sends[i].wait_recv()
-        total[...] += landed[i].astype(jnp.float32)
+        flush()
+        waiting.append(sends[slot])
+
+    steps = list(range(1, far)) + [0]
+    for step in steps:
+        send(far + step, own_sum(step, at.across_row, []), at.second)
+    for step in steps:
+        send(step, own_sum(step, at.second_row, []), at.second)
+    flush()
+    for step in steps:
+        send(2 * far + step, own_sum(step, at.first_row, [far + step]), at.first)
+    flush()
+    for step in steps[:-1]:
+        value = own_sum(step, at.own_row, [step, 2 * far + step])
+        send(3 * far + step - 1, value, at.block(step, at.own_row))
+    flush()
+    total[...] = resid_ref[...].astype(jnp.float32) + own_sum(0, at.own_row, [0, 2 * far])
+    for step in steps[:-1]:
+        sends[3 * far + step - 1].wait_recv()
+        total[...] += landed[3 * far + step - 1].astype(jnp.float32)
     out_ref[...] = total[...].astype(out_ref.dtype)
-    for send in sends:
-        send.wait_send()
+    for copy in sends.values():
+        copy.wait_send()
     for pair in pairs:
         pair.wait_send()
 
@@ -268,6 +343,72 @@
         compiler_params=pltpu.CompilerParams(collective_id=1, has_side_effects=True),
         name="scatter_rows",
     )(terms, resid)
+
+
+def branch_kernel(
+    stride, width, steps, x_ref, dg_ref, du_ref, dd_ref, eg_ref, eu_ref, ed_ref, out_ref, total
+):
+    me = lax.axis_index("ep")
+    step = pl.program_id(1)
+    x = x_ref[:, :width]
+    scales = x_ref[:, width:].astype(jnp.float32)
+    column = lax.broadcasted_iota(jnp.int32, scales.shape, 1)
+
+    def scale_of(owner):
+        held = (column == owner) | (column == owner + stride) | (column == owner + 2 * stride)
+        return jnp.sum(jnp.where(held, scales, 0.0), axis=1, keepdims=True)
+
+    def branch(w_gate, w_up, w_down, scale):
+        gate_part = jnp.dot(x, w_gate, preferred_element_type=jnp.float32)
+        up_part = jnp.dot(x, w_up, preferred_element_type=jnp.float32)
+        hidden = (scale * jax.nn.silu(gate_part) * up_part).astype(jnp.bfloat16)
+        return jnp.dot(hidden, w_down, preferred_element_type=jnp.float32)
+
+    terms = branch(dg_ref[...], du_ref[...], dd_ref[...], scale_of(stride - 1))
+    terms = terms + branch(eg_ref[0], eu_ref[0], ed_ref[0], scale_of(me))
+    if steps > 1:
+
+        @pl.when(step == 0)
+        def _():
+            total[...] = terms
+
+        @pl.when(step > 0)
+        def _():
+            total[...] += terms
+
+        @pl.when(step == steps - 1)
+        def _():
+            out_ref[...] = total[...].astype(out_ref.dtype)
+    else:
+        out_ref[...] = terms.astype(out_ref.dtype)
+
+
+def branch_terms(gathered, width, stride, dense, expert):
+    count = gathered.shape[0]
+    dense_units, expert_units = dense[0].shape[1], expert[0].shape[2]
+    steps = 2 if dense_units % 256 == 0 and expert_units % 256 == 0 else 1
+    tile = 512 if count % 512 == 0 else count
+    dense_tile, expert_tile = dense_units // steps, expert_units // steps
+    dense_in = pl.BlockSpec((width, dense_tile), lambda r, j: (0, j))
+    expert_in = pl.BlockSpec((1, width, expert_tile), lambda r, j: (0, 0, j))
+    return pl.pallas_call(
+        functools.partial(branch_kernel, stride, width, steps),
+        grid=(count // tile, steps),
+        out_shape=jax.ShapeDtypeStruct((count, width), jnp.bfloat16),
+        in_specs=[
+            pl.BlockSpec((tile, gathered.shape[1]), lambda r, j: (r, 0)),
+            dense_in,
+            dense_in,
+            pl.BlockSpec((dense_tile, width), lambda r, j: (j, 0)),
+            expert_in,
+            expert_in,
+            pl.BlockSpec((1, expert_tile, width), lambda r, j: (0, j, 0)),
+        ],
+        out_specs=pl.BlockSpec((tile, width), lambda r, j: (r, 0)),
+        scratch_shapes=[pltpu.VMEM((tile, width), jnp.float32)],
+        compiler_params=pltpu.CompilerParams(vmem_limit_bytes=50 * 1024 * 1024),
+        name="branch_terms",
+    )(gathered, *dense, *expert)
 
 
 def in_pieces(values):
@@ -333,25 +474,14 @@
     scales = jnp.pad(scales, ((0, 0), (0, -scales.shape[1] % 128)))
     gathered = gather_rows(jnp.concatenate([normed, scales], axis=1), n)
     gathered = gathered.reshape(n * rows, -1)
-    piece, scales = gathered[:, :width], gathered[:, width:].astype(jnp.float32)
-    stride = expert_count + 1
-    column = jnp.arange(scales.shape[1], dtype=jnp.int32)
-    owner = jnp.where(column < 3 * stride, column % stride, stride)
-    me = lax.axis_index("ep")
-    own_weight = jnp.sum(jnp.where(owner == me, scales, 0.0), axis=1, keepdims=True)
-    branch_all = jnp.sum(jnp.where(owner == expert_count, scales, 0.0), axis=1, keepdims=True)
-
-    def hidden_units(w_gate, w_up, scale):
-        gate_part = jnp.dot(piece, w_gate, preferred_element_type=jnp.float32)
-        up_part = jnp.dot(piece, w_up, preferred_element_type=jnp.float32)
-        return (scale * jax.nn.silu(gate_part) * up_part).astype(jnp.bfloat16)
-
-    dense_hidden = hidden_units(dense_gate, dense_up, branch_all)
-    expert_hidden = hidden_units(expert_gate[0], expert_up[0], own_weight)
-    terms = jnp.dot(dense_hidden, dense_down, preferred_element_type=jnp.float32) + jnp.dot(
-        expert_hidden, expert_down[0], preferred_element_type=jnp.float32
-    )
-    layer_out = scatter_rows(terms.astype(jnp.bfloat16).reshape(n, rows, width), resid)
+    terms = branch_terms(
+        gathered,
+        width,
+        expert_count + 1,
+        (dense_gate, dense_up, dense_down),
+        (expert_gate, expert_up, expert_down),
+    )
+    layer_out = scatter_rows(terms.reshape(n, rows, width), resid)
     return (layer_out, new_state)
 
 

time: 111 us -> 84.9 us (0.76)
  matrix products: 30.6 us -> 12.7 us
  Pallas kernels: 66.7 us -> 57.8 us
  local copies, waits for them, and re-layouts: 4.38 us -> 6.77 us
  other arithmetic: 7.63 us -> 5.98 us
    dot_general x4 -> x0, matrix products: 19.6 us -> none  [the longest x1 7.56 us: on_device(): jnp.dot(expert_hidden, expert_down[0], preferred_element_type=jnp.float32)]
    pallas_call x0 -> x1, Pallas kernels: none -> 11.8 us  [branch_terms(): pl.pallas_call(functools.partial(branch_kernel, stride, width, steps), gr...]
    pallas_call x1, Pallas kernels: 35.6 us -> 25.2 us  [gather_rows(): pl.pallas_call(functools.partial(gather_kernel, chips), out_shape=jax.Sha...]
    pallas_call x1, Pallas kernels: 31.1 us -> 20.8 us  [scatter_rows(): pl.pallas_call(functools.partial(scatter_kernel, chips), out_shape=jax.Sh...]
    unnamed x45 -> x35, local copies, waits for them, and re-layouts: 1.6 us -> 4 us
where the time goes in v2:
time: 84.9 us; the launch traced here: 84.2 us
  Pallas kernels  57.8 us (68%)
  matrix products  12.7 us (15%)
  local copies, waits for them, and re-layouts  6.77 us (8%)
  other arithmetic  5.98 us (7%)
  between operations  0.95 us (1%)
    pallas_call x1, Pallas kernels, gather_rows(): pl.pallas_call(functools.partial(gather_kernel, chips), out_shape=jax.Sha...  25.2 us
    pallas_call x1, Pallas kernels, scatter_rows(): pl.pallas_call(functools.partial(scatter_kernel, chips), out_shape=jax.Sh...  20.8 us
    pallas_call x1, Pallas kernels, branch_terms(): pl.pallas_call(functools.partial(branch_kernel, stride, width, steps), gr...  11.8 us
    unnamed x35, local copies, waits for them, and re-layouts  4 us
    dot_general x1, matrix products, state_mixer(): jnp.dot(normed_in, w_drive, preferred_element_type=jnp.float32)  2.06 us
    dot_general x1, matrix products, state_mixer(): jnp.dot(mixed, w_output, preferred_element_type=jnp.float32)  1.72 us

profile of v2, /device:TPU:0, one launch (start us, length us, event | category | flops | bytes accessed | tf_op | source)
XLA Modules:
  0.0 84.2 jit_solution(8665284179069383127)
XLA Ops:
  0.6 0.0 copy-start
  0.7 0.0 copy-start.5
  0.7 0.8 exp.18
  1.5 1.0 %fusion.25 = f32[16]{0:T(128)S(1)} fusion(bf16[16,2048]{1,0:T(8,128)(2,1)} %param.26), kind=kLoop, calls=%fused_computation.39 | loop fusion | flops 98288 | bytes 65600 | tf_op jit(solution)/shard_map/reduce_sum | solution.py:16
  2.5 1.3 %fusion.37 = pred[16,32]{1,0:T(8,128)(4,1)} fusion(s32[16,6]{0,1:T(8,128)} %param.44), kind=kLoop, calls=%fused_computation.53 | loop fusion | flops 5632 | bytes 896 | tf_op jit(solution)/shard_map/reduce_or | solution.py:90
  3.9 2.1 %convolution_convert_fusion = bf16[16,512]{1,0:T(8,128)(2,1)S(1)} fusion(bf16[2048,512]{1,0:T(8,128)(2,1)} %param.29, bf16[16,2048]{1,0:T(8,128)(2,1)} %param.26, f32[2048]{0:T(1024)} %param.28, f32[16]{0:T(128)S(1)} %add_rsqrt_fusion.1), kind=kOutput, calls=%fused_computation.14 | convolution fusion | flops 33693696 | bytes 2187328 | tf_op jit(solution)/shard_map/dot_general | solution.py:41
  5.9 0.0 copy-done.14
  6.0 0.8 cosine_multiply_fusion
  6.7 0.1 reshape.53
  6.9 0.1 reshape_squeeze.6
  7.0 0.1 reshape_squeeze.7
  7.2 1.3 %fusion.3 = f32[16,32,64]{2,0,1:T(8,128)S(1)} fusion(f32[32,64,16]{1,2,0:T(8,128)S(1)} %copy-done.5, f32[32,64,16]{1,2,0:T(8,128)S(1)} %copy-done.4, f32[16,32,64]{2,1,0:T(8,128)S(1)} %reshape_squeeze.7, f32[16,32,64]{2,1,0:T(8,128)S(1)} %reshape_squeeze.6, f32[32,64]{1,0:T(8,128)} %get-tuple-element.6, f32[32,64]{1,0:T(8,128)} %get-tuple-element.7, ...), kind=kOutput, calls=%fused_computation.6 | convolution fusion | flops 6520832 | bytes 704512 | tf_op jit(solution)/shard_map/gpc,sgc->sgp/dot_general | solution.py:54
  8.4 1.5 %fusion.4 = f32[16,32,64]{2,0,1:T(8,128)S(1)} fusion(f32[32,64,16]{1,2,0:T(8,128)S(1)} %copy-done.4, f32[32,64,16]{1,2,0:T(8,128)} %param.33, f32[16,32,64]{2,1,0:T(8,128)S(1)} %reshape_squeeze.7, f32[16,32,64]{2,1,0:T(8,128)S(1)} %reshape_squeeze.6, f32[32,64]{1,0:T(8,128)} %get-tuple-element.6, f32[32,64]{1,0:T(8,128)} %get-tuple-element.7, ...), kind=kOutput, calls=%fused_computation.8 | convolution fusion | flops 6520832 | bytes 704512 | tf_op jit(solution)/shard_map/gpc,sgc->sgp/dot_general | solution.py:53
  9.9 0.1 copy.59
  10.0 0.8 stack_reshape.6
  10.8 1.5 %fusion.58 = f32[32,16,16]{2,1,0:T(8,128)S(1)} fusion(f32[16,32,64]{2,0,1:T(8,128)S(1)} %fusion.4, f32[32,16,64]{2,1,0:T(8,128)} %param.35), kind=kOutput, calls=%fused_computation.92 | convolution fusion | flops 6291456 | bytes 294912 | tf_op jit(solution)/shard_map/xej,fxj->fxe/dot_general | solution.py:59
  12.4 0.0 copy-start.6
  12.4 1.5 %fusion.2 = f32[16,32,16]{2,0,1:T(8,128)S(1)} fusion(f32[32,16,16]{2,1,0:T(8,128)S(1)} %fusion.58, f32[16,32,64]{2,0,1:T(8,128)S(1)} %fusion.3, f32[32,16,64]{2,1,0:T(8,128)} %param.36), kind=kOutput, calls=%fused_computation.4 | convolution fusion | flops 6299648 | bytes 327680 | tf_op jit(solution)/shard_map/xej,fxj->fxe/dot_general | solution.py:61
  13.9 0.1 copy.60
  14.0 0.1 stack_reshape.7
  14.1 1.6 %pad_maximum_fusion = f32[2,16,2048]{2,1,0:T(8,128)} fusion(f32[1,16,2048]{2,1,0:T(8,128)S(1)} %stack_reshape.7, f32[1,16,2048]{2,1,0:T(8,128)} %stack_reshape.6), kind=kLoop, calls=%fused_computation.25 | loop fusion | flops 65536 | bytes 524288 | tf_op jit(solution)/shard_map/stack | solution.py:71
  15.7 0.1 copy.54
  15.8 0.2 reshape.54
  16.1 0.2 fusion.59
  16.2 1.7 %fusion.22 = (f32[16]{0:T(128)S(1)}, bf16[16,2048]{1,0:T(8,128)(2,1)S(1)}) fusion(bf16[512,2048]{1,0:T(8,128)(2,1)S(1)} %copy-done, f32[16,512]{1,0:T(8,128)S(1)} %fusion.59, bf16[16,512]{1,0:T(8,128)(2,1)S(1)} %fusion.45, bf16[512,512]{1,0:T(8,128)(2,1)} %param.39, bf16[16,2048]{1,0:T(8,128)(2,1)S(1)} %copy-done.6), kind=kOutput, calls=%fused_computation.36 | convolution fusion | flops 42180592 | bytes 2801728 | tf_op jit(solution)/shard_map/dot_general | solution.py:69
  18.0 0.0 copy-start.7
  18.0 0.0 copy-start.1
  18.0 0.1 fusion.24
  18.1 0.9 %fusion.15 = f32[16,1]{0,1:T(1,128)S(1)} fusion(bf16[16,2048]{1,0:T(8,128)(2,1)S(1)} %fusion.24, f32[2048,1]{0,1:T(1,128)} %bitcast.53), kind=kOutput, calls=%fused_computation.24 | convolution fusion | flops 393264 | bytes 73792 | tf_op jit(solution)/shard_map/dot_general | solution.py:471
  19.0 0.9 %fusion.57 = (f32[16]{0:T(128)S(1)}, f32[16,4]{0,1:T(4,128)S(1)}) fusion(bf16[16,2048]{1,0:T(8,128)(2,1)S(1)} %fusion.24, bf16[2048,4]{0,1:T(4,128)(2,1)} %param.42), kind=kOutput, calls=%fused_computation.91 | convolution fusion | flops 262192 | bytes 82240 | tf_op jit(solution)/shard_map/dot_general | solution.py:82
  19.9 0.1 copy.58
  20.0 1.1 %convolution_exponential_fusion = f32[16,32]{1,0:T(8,128)S(1)} fusion(bf16[16,2048]{1,0:T(8,128)(2,1)S(1)} %fusion.24, bf16[2048,32]{0,1:T(8,128)(2,1)} %param.43), kind=kOutput, calls=%fused_computation.17 | convolution fusion | flops 2097152 | bytes 198656 | tf_op jit(solution)/shard_map/dot_general | solution.py:84
  21.1 0.1 copy.57
  21.2 0.1 copy.55
  21.2 0.1 fusion.10
  21.3 0.1 copy.56
  21.4 0.1 select_reduce_fusion
  21.5 0.1 divide_select_fusion
  21.6 0.1 reduce-precision_convert_fusion.1
  21.7 0.1 fusion.54
  21.8 0.6 pad_maximum_fusion.1.own_ref
  22.4 25.2 %gather_rows.1 = bf16[32,16,2176]{2,1,0:T(8,128)(2,1)} custom-call(bf16[16,2176]{1,0:T(8,128)(2,1)} %pad_maximum_fusion.1.own_ref), custom_call_target="tpu_custom_call" | custom-call | bytes 60000000 | tf_op jit(solution)/shard_map/gather_rows/pallas_call | solution.py:219
  47.6 0.0 copy-start.2
  47.7 1.2 %copy-done.2 = bf16[2048,256]{1,0:T(8,128)(2,1)S(1)} copy-done((bf16[2048,256]{1,0:T(8,128)(2,1)S(1)}, bf16[2048,256]{1,0:T(8,128)(2,1)}, u32[]{:S(2)}) %copy-start.2) | copy-done | bytes 1048600
  48.9 1.2 %copy-done.3 = bf16[256,2048]{1,0:T(8,128)(2,1)S(1)} copy-done((bf16[256,2048]{1,0:T(8,128)(2,1)S(1)}, bf16[256,2048]{1,0:T(8,128)(2,1)}, u32[]{:S(2)}) %copy-start.3) | copy-done | bytes 1048600
  50.1 11.8 %branch_terms.1 = bf16[512,2048]{1,0:T(8,128)(2,1)} custom-call(bf16[512,2176]{1,0:T(8,128)(2,1)} %bitcast.51, bf16[2048,256]{1,0:T(8,128)(2,1)S(1)} %copy-done.1, bf16[2048,256]{1,0:T(8,128)(2,1)S(1)} %copy-done.2, bf16[256,2048]{1,0:T(8,128)(2,1)S(1)} %copy-done.3, bf16[1,2048,512]{2,1,0:T(8,128)(2,1)} %eg_ref.1, bf16[1,2048,512]{2,1,0:T(8,128)(2,1)} %eu_ref.1, ...), custom_call_target="tpu_custom_call" | custom-call | tf_op jit(solution)/shard_map/branch_terms/pallas_call | solution.py:394
  61.9 20.8 %scatter_rows.1 = bf16[16,2048]{1,0:T(8,128)(2,1)} custom-call(bf16[32,16,2048]{2,1,0:T(8,128)(2,1)} %bitcast.52, bf16[16,2048]{1,0:T(8,128)(2,1)} %copy-done.7), custom_call_target="tpu_custom_call" | custom-call | tf_op jit(solution)/shard_map/scatter_rows/pallas_call | solution.py:328
  82.7 1.5 %copy.70 = bf16[16,2048]{1,0:T(8,128)(2,1)} copy(bf16[16,2048]{1,0:T(8,128)(2,1)} %scatter_rows.1) | data formatting | bytes 131072
  (31 shorter events, 0.1 us)
Async XLA Ops:
  0.6 15.6 %copy-start = (bf16[512,2048]{1,0:T(8,128)(2,1)S(1)}, bf16[512,2048]{1,0:T(8,128)(2,1)}, u32[]{:S(2)}) copy-start(bf16[512,2048]{1,0:T(8,128)(2,1)} %param.40) | copy-start | bytes 6291460
  0.6 6.5 %copy-start.4 = (f32[32,64,16]{1,2,0:T(8,128)S(1)}, f32[32,64,16]{1,2,0:T(8,128)}, u32[]{:S(2)}) copy-start(f32[32,64,16]{1,2,0:T(8,128)} %param.34) | copy-start | bytes 393220
  0.7 6.5 %copy-start.5 = (f32[32,64,16]{1,2,0:T(8,128)S(1)}, f32[32,64,16]{1,2,0:T(8,128)}, u32[]{:S(2)}) copy-start(f32[32,64,16]{1,2,0:T(8,128)} %param.33) | copy-start | bytes 393220
  0.7 5.3 %copy-start.13 = (f32[32,64]{1,0:T(8,128)S(1)}, f32[32,64]{1,0:T(8,128)}, u32[]{:S(2)}) copy-start(f32[32,64]{1,0:T(8,128)} %param.31) | copy-start | bytes 24580
  0.7 5.3 %copy-start.14 = (f32[32,64]{1,0:T(8,128)S(1)}, f32[32,64]{1,0:T(8,128)}, u32[]{:S(2)}) copy-start(f32[32,64]{1,0:T(8,128)} %param.30) | copy-start | bytes 24580
  0.7 6.2 %copy-start.9 = (f32[2,16,2048]{2,1,0:T(8,128)S(1)}, f32[2,16,2048]{2,1,0:T(8,128)}, u32[]{:S(2)}) copy-start(f32[2,16,2048]{2,1,0:T(8,128)} %param.27) | copy-start | bytes 786436
  6.0 0.8 copy-start.10
  10.8 5.2 %copy-start.11 = (bf16[16,512]{1,0:T(8,128)(2,1)S(1)}, bf16[16,512]{1,0:T(8,128)(2,1)}, u32[]{:S(2)}) copy-start(bf16[16,512]{1,0:T(8,128)(2,1)} %copy-done.10) | copy-start | bytes 49156
  10.8 5.2 %copy-start.16 = (f32[512]{0:T(512)S(1)}, f32[512]{0:T(512)}, u32[]{:S(2)}) copy-start(f32[512]{0:T(512)} %param.37) | copy-start | bytes 6148
  10.8 5.2 %copy-start.8 = (bf16[512,512]{1,0:T(8,128)(2,1)S(1)}, bf16[512,512]{1,0:T(8,128)(2,1)}, u32[]{:S(2)}) copy-start(bf16[512,512]{1,0:T(8,128)(2,1)} %param.38) | copy-start | bytes 1572868
  12.4 3.9 %copy-start.6 = (bf16[16,2048]{1,0:T(8,128)(2,1)S(1)}, bf16[16,2048]{1,0:T(8,128)(2,1)}, u32[]{:S(2)}) copy-start(bf16[16,2048]{1,0:T(8,128)(2,1)} %param.26) | copy-start | bytes 196612
  15.7 2.2 %copy-start.15 = (f32[2048]{0:T(1024)S(1)}, f32[2048]{0:T(1024)}, u32[]{:S(2)}) copy-start(f32[2048]{0:T(1024)} %param.41) | copy-start | bytes 24580
  16.0 5.4 %copy-start.12 = (pred[16,32]{1,0:T(8,128)(4,1)S(1)}, pred[16,32]{1,0:T(8,128)(4,1)}, u32[]{:S(2)}) copy-start(pred[16,32]{1,0:T(8,128)(4,1)} %fusion.37) | copy-start | bytes 1540
  18.0 43.9 %copy-start.7 = (bf16[16,2048]{1,0:T(8,128)(2,1)}, bf16[16,2048]{1,0:T(8,128)(2,1)S(1)}, u32[]{:S(2)}) copy-start(bf16[16,2048]{1,0:T(8,128)(2,1)S(1)} %get-tuple-element.12.resid_ref) | copy-start | bytes 196612
  18.0 29.7 %copy-start.1 = (bf16[2048,256]{1,0:T(8,128)(2,1)S(1)}, bf16[2048,256]{1,0:T(8,128)(2,1)}, u32[]{:S(2)}) copy-start(bf16[2048,256]{1,0:T(8,128)(2,1)} %dg_ref.1) | copy-start | bytes 3145732
  47.6 1.2 %copy-start.2 = (bf16[2048,256]{1,0:T(8,128)(2,1)S(1)}, bf16[2048,256]{1,0:T(8,128)(2,1)}, u32[]{:S(2)}) copy-start(bf16[2048,256]{1,0:T(8,128)(2,1)} %du_ref.1) | copy-start | bytes 3145732
  48.9 1.2 %copy-start.3 = (bf16[256,2048]{1,0:T(8,128)(2,1)S(1)}, bf16[256,2048]{1,0:T(8,128)(2,1)}, u32[]{:S(2)}) copy-start(bf16[256,2048]{1,0:T(8,128)(2,1)} %dd_ref.1) | copy-start | bytes 3145732
